TPU v7x, 32 devices: a whole 2x2x4 slice. The times are simulated.
32 devices in a mesh: sp: 8 (over z, x), tp: 4 (over y, core).
Axes of the slice: x: 2, y: 2, z: 4, core: 2. Of those that a mesh axis runs over, the one named last changes fastest.
Arguments:
- tokens: bfloat16 [8192, 2048], P('sp', 'tp'), may hold values from -70 to 70
- w_query: bfloat16 [2048, 1024], P(None, 'tp'), may hold values from -0.125 to 0.125
- w_key: bfloat16 [2048, 1024], P(None, 'tp'), may hold values from -0.125 to 0.125
- w_value: bfloat16 [2048, 1024], P(None, 'tp'), may hold values from -0.125 to 0.125
- w_delta_gate: bfloat16 [2048, 1024], P(None, 'tp'), may hold values from -0.125 to 0.125
- w_glu_value: bfloat16 [2048, 1024], P(None, 'tp'), may hold values from -0.125 to 0.125
- w_glu_gate: bfloat16 [2048, 1024], P(None, 'tp'), may hold values from -0.125 to 0.125
- w_conv_gate: bfloat16 [2048, 1024], P(None, 'tp'), may hold values from -0.125 to 0.125
- w_beta: bfloat16 [2048, 8], replicated, may hold values from -0.125 to 0.125
- w_decay: bfloat16 [2048, 8], replicated, may hold values from -0.125 to 0.125
- decay_log: float32 [8], replicated, may hold values from -12 to -3
- head_gain: float32 [128], replicated, may hold values from 0.1 to 1.9
- conv_taps: bfloat16 [31, 1024], P(None, 'tp'), may hold values from -2.5 to 2.5
- ln_gain: float32 [1024], P('tp'), may hold values from 0.1 to 1.9
- ln_shift: float32 [1024], P('tp'), may hold values from -3 to 3
- out_delta: bfloat16 [1024, 2048], P('tp'), may hold values from -0.125 to 0.125
- out_conv: bfloat16 [1024, 2048], P('tp'), may hold values from -0.125 to 0.125
Outputs:
- mixed_out: bfloat16 [8192, 2048], P(('sp', 'tp'))
All inputs are finite; a program needn't handle non-finite values.
Results may differ from a plain program's by a relative error of at most 0.024.
Values may be sent and summed in bfloat16 or wider, within the bound.
A program may use at most 64 MiB of HBM per device.

v0:
```python
import jax
import jax.numpy as jnp
from jax import lax
from jax.sharding import PartitionSpec as P

SPAN = 64
TINY_NORM = 1e-06
TINY_VAR = 1e-05
HIGHEST = lax.Precision.HIGHEST


def entering(part, axis, combine, identity):
    place = lax.axis_index(axis)
    gathered = lax.all_gather(part, axis)
    state = jnp.zeros_like(part) + jnp.asarray(identity, part.dtype)

    def one(hop, state):
        return combine(state, lax.dynamic_index_in_dim(gathered, hop, 0, False))

    return lax.fori_loop(0, place, one, state)


def shifted(block, axis, distance):
    devices = range(lax.axis_size(axis))
    route = [(i - distance, i) for i in devices if i - distance in devices]
    return lax.ppermute(block, axis, route)


def block_terms(query, keys, values, strength, log_decay):
    log_sum = jnp.cumsum(log_decay, axis=-1)
    offsets = jnp.arange(SPAN)
    causal = offsets[:, None] >= offsets[None, :]
    strict = offsets[:, None] > offsets[None, :]
    spread = log_sum[..., :, None] - log_sum[..., None, :]
    damping = jnp.where(causal, jnp.exp(jnp.where(causal, spread, 0.0)), 0.0)
    scaled_keys = keys * strength[..., None]
    lower = jnp.where(
        strict, jnp.einsum("hnid,hnjd->hnij", scaled_keys, keys, precision=HIGHEST) * damping, 0.0
    )
    identity = jnp.eye(SPAN, dtype=jnp.float32)
    right = jnp.concatenate(
        [values * strength[..., None], scaled_keys * jnp.exp(log_sum)[..., None]], axis=-1
    )
    solved = jax.scipy.linalg.solve_triangular(
        identity + lower, right, lower=True, unit_diagonal=True
    )
    width = values.shape[-1]
    scores = jnp.einsum("hnid,hnjd->hnij", query, keys, precision=HIGHEST) * damping
    return (log_sum, solved[..., :width], solved[..., width:], scores)


def local(
    tokens,
    w_query,
    w_key,
    w_value,
    w_delta_gate,
    w_glu_value,
    w_glu_gate,
    w_conv_gate,
    w_beta,
    w_decay,
    decay_log,
    head_gain,
    conv_taps,
    ln_gain,
    ln_shift,
    out_delta,
    out_conv,
):
    rows_here = tokens.shape[0]
    tp_size = lax.axis_size("tp")
    width_all = tokens.shape[1] * tp_size
    weights = (
        w_query,
        w_key,
        w_value,
        w_delta_gate,
        w_glu_value,
        w_glu_gate,
        w_conv_gate,
        w_beta,
        w_decay,
    )
    piece = lax.all_gather(tokens, "tp", axis=1, tiled=True)
    totals = tuple(
        (jnp.dot(piece, weight, preferred_element_type=jnp.float32) for weight in weights)
    )
    squares = jnp.sum(jnp.square(piece.astype(jnp.float32)), axis=1)
    sums, squares = (totals, squares)
    inv_rms = lax.rsqrt(squares / width_all + TINY_NORM)[:, None]
    scaled = [summed * inv_rms for summed in sums]
    query_raw, key_raw, value_raw, delta_gate_raw, glu_value_raw, glu_gate_raw, conv_gate_raw = [
        item.astype(jnp.bfloat16) for item in scaled[:7]
    ]
    head_size = head_gain.shape[0]
    heads_here = w_query.shape[1] // head_size
    first_head = lax.axis_index("tp") * heads_here
    strength = jax.nn.sigmoid(lax.dynamic_slice_in_dim(scaled[7], first_head, heads_here, 1))
    rates = jnp.exp(lax.dynamic_slice_in_dim(decay_log, first_head, heads_here, 0))
    log_decay = -rates[None, :] * jax.nn.softplus(
        lax.dynamic_slice_in_dim(scaled[8], first_head, heads_here, 1)
    )
    blocks = rows_here // SPAN

    def to_blocks(raw):
        return jnp.transpose(raw.reshape(blocks, SPAN, heads_here, head_size), (2, 0, 1, 3))

    def unit_rows(array):
        return array * lax.rsqrt(jnp.sum(array * array, axis=-1, keepdims=True) + TINY_NORM)

    query = unit_rows(to_blocks(query_raw.astype(jnp.float32))) * head_size ** (-0.5)
    keys = unit_rows(to_blocks(key_raw.astype(jnp.float32)))
    values = to_blocks(value_raw.astype(jnp.float32))
    strength_blocks = jnp.transpose(strength.reshape(blocks, SPAN, heads_here), (2, 0, 1))
    decay_blocks = jnp.transpose(log_decay.reshape(blocks, SPAN, heads_here), (2, 0, 1))
    log_sum, corrected, key_terms, scores = block_terms(
        query, keys, values, strength_blocks, decay_blocks
    )

    def advance(memory, inputs):
        query_block, keys_block, corrected_block, terms_block, scores_block, log_block = inputs
        extended = jnp.concatenate([jnp.zeros_like(corrected_block), corrected_block], axis=-1)
        fresh = extended - jnp.einsum("hcd,hde->hce", terms_block, memory, precision=HIGHEST)
        output = jnp.einsum(
            "hcd,hde->hce", query_block * jnp.exp(log_block)[..., None], memory, precision=HIGHEST
        )
        output = output + jnp.einsum("hcs,hse->hce", scores_block, fresh, precision=HIGHEST)
        tail_log = log_block[:, -1:]
        weighted = keys_block * jnp.exp(tail_log - log_block)[..., None]
        memory = memory * jnp.exp(tail_log)[..., None] + jnp.einsum(
            "hcd,hce->hde", weighted, fresh, precision=HIGHEST
        )
        return (memory, output)

    start_state = jnp.concatenate(
        [
            jnp.broadcast_to(
                jnp.eye(head_size, dtype=jnp.float32), (heads_here, head_size, head_size)
            ),
            jnp.zeros((heads_here, head_size, head_size), jnp.float32),
        ],
        axis=-1,
    )
    sequence_inputs = tuple(
        (jnp.moveaxis(item, 1, 0) for item in (query, keys, corrected, key_terms, scores, log_sum))
    )
    final, outputs = lax.scan(advance, start_state, sequence_inputs)
    outputs = jnp.moveaxis(outputs, 0, 1).reshape(heads_here, rows_here, 2 * head_size)

    def compose(earlier, later):
        moved = jnp.einsum("hij,hjk->hik", later[..., :head_size], earlier, precision=HIGHEST)
        return moved + jnp.concatenate(
            [jnp.zeros_like(later[..., :head_size]), later[..., head_size:]], axis=-1
        )

    prefix = entering(final, "sp", compose, start_state)
    carried = prefix[..., head_size:]
    result = outputs[..., head_size:] + jnp.einsum(
        "htd,hde->hte", outputs[..., :head_size], carried, precision=HIGHEST
    )
    result = jnp.transpose(result, (1, 0, 2))
    result = (
        result
        * lax.rsqrt(jnp.mean(result * result, axis=-1, keepdims=True) + TINY_NORM)
        * head_gain
    )
    delta_mixed = (
        result.reshape(rows_here, heads_here * head_size)
        * jax.nn.silu(delta_gate_raw.astype(jnp.float32))
    ).astype(jnp.bfloat16)
    kernel = conv_taps.shape[0]
    channels = conv_taps.shape[1]
    gated_units = (
        glu_value_raw.astype(jnp.float32) * jax.nn.sigmoid(glu_gate_raw.astype(jnp.float32))
    ).astype(jnp.bfloat16)
    before = shifted(gated_units[rows_here - (kernel - 1) :], "sp", 1)
    padded = jnp.concatenate([before, gated_units], axis=0)
    filtered = jnp.zeros((rows_here, channels), jnp.float32)
    for offset in range(kernel):
        filtered = filtered + padded[offset : offset + rows_here].astype(jnp.float32) * conv_taps[
            offset
        ].astype(jnp.float32)
    first_sum = jnp.sum(filtered, axis=1)
    second_sum = jnp.sum(filtered * filtered, axis=1)
    first_sum, second_sum = lax.psum((first_sum, second_sum), "tp")
    channels_all = channels * tp_size
    center = first_sum / channels_all
    variance = jnp.maximum(second_sum / channels_all - center * center, 0.0)
    normed = (filtered - center[:, None]) * lax.rsqrt(variance + TINY_VAR)[
        :, None
    ] * ln_gain + ln_shift
    conv_mixed = (jax.nn.silu(normed) * jax.nn.silu(conv_gate_raw.astype(jnp.float32))).astype(
        jnp.bfloat16
    )
    summed = jnp.dot(delta_mixed, out_delta, preferred_element_type=jnp.float32)
    return lax.psum_scatter(
        (summed + jnp.dot(conv_mixed, out_conv, preferred_element_type=jnp.float32)).astype(
            jnp.bfloat16
        ),
        "tp",
        scatter_dimension=0,
        tiled=True,
    )


def solution(mesh):
    return jax.shard_map(
        local,
        mesh=mesh,
        in_specs=(
            P("sp", "tp"),
            P(None, "tp"),
            P(None, "tp"),
            P(None, "tp"),
            P(None, "tp"),
            P(None, "tp"),
            P(None, "tp"),
            P(None, "tp"),
            P(),
            P(),
            P(),
            P(),
            P(None, "tp"),
            P("tp"),
            P("tp"),
            P("tp", None),
            P("tp", None),
        ),
        out_specs=P(("sp", "tp"), None),
        check_vma=False,
    )
```

profile of v0, /device:TPU:0, one launch (start us, length us, event | category | flops | bytes accessed | tf_op | source)
XLA Modules:
  0.0 483.8 jit_solution(3299517887842109902)
XLA Ops:
  9.5 36.6 %all-gather.4.cloned.1.call-done = bf16[1024,2048]{1,0:T(8,128)(2,1)} async-done(((bf16[1024,512]{1,0:T(8,128)(2,1)}), bf16[1024,2048]{1,0:T(8,128)(2,1)}) %all-gather.4.cloned.1.call-update) | async-done | bytes 4194320 | tf_op jit(solution)/shard_map/all_gather | solution.py:85
  46.1 3.2 multiply_reduce_fusion
  52.8 3.4 fusion.45
  57.8 3.7 fusion.47
  62.4 4.7 fusion.43
  69.9 3.8 fusion.39
  73.7 158.7 %custom-call.4 = f32[2,16,1,64,64]{3,4,2,1,0:T(8,128)} custom-call(f32[2,16,1,64,64]{4,3,2,1,0:T(8,128)} %fusion.39), custom_call_target="InvertDiagBlocksLowerTriangular" | custom-call | tf_op jit(solution)/shard_map/jit(_solve_triangular)/vmap(vmap())/triangular_solve | solution.py:44
  232.4 2.1 bitcast_multiply_fusion.7
  234.5 2.0 fusion.16
  240.8 3.1 fusion.26
  243.9 104.2 %while.22 = (s32[]{:T(128)}, f32[2,128,256]{2,1,0:T(8,128)S(1)}, f32[16,2,64,256]{3,2,1,0:T(8,128)}, f32[16,2,64]{2,0,1:T(8,128)S(1)}, f32[16,2,64,128]{3,2,1,0:...) while((s32[]{:T(128)}, f32[2,128,256]{2,1,0:T(8,128)S(1)}, ...), condition=%wide.region_5.6_spmd, body=%wide.region_4.5_spmd.sunk | while | flops 176390272 | bytes 2298537 | solution.py:148
  248.7 1.8 fusion.190
  261.7 1.8 fusion.190
  268.3 1.8 fusion.190
  274.8 1.8 fusion.190
  281.3 1.8 fusion.190
  294.3 1.8 fusion.190
  300.8 1.8 fusion.190
  313.8 1.8 fusion.190
  326.9 1.8 fusion.190
  333.4 1.8 fusion.190
  346.4 1.8 fusion.190
  349.0 3.6 fusion.58
  354.8 3.5 collective-permute-start
  358.9 1.8 copy.62
  360.8 6.0 %fusion.142 = (f32[1024]{0:T(1024)S(1)}, f32[1024]{0:T(1024)S(1)}, f32[1024,256]{1,0:T(8,128)}) fusion(f32[256]{0:T(256)S(1)} %bitcast.215, bf16[1024,256]{1,0:T(8,128)(2,1)S(1)} %copy-done.10, f32[256]{0:T(256)S(1)} %bitcast.216, bf16[30,256]{1,0:T(8,128)(2,1)S(1)} %collective-permute-done, f32[256]{0:T(256)S(1)} %bitcast.187, f32[256]{0:T(256)S(1)} %bitcast.188, ...), kind=kLoop, calls=%fused_computation.252 | loop fusion | flops 48494592 | bytes 1628160 | tf_op jit(solution)/shard_map/reduce_sum | solution.py:184
  366.8 6.3 %all-reduce.3 = (f32[1024]{0:T(1024)S(1)}, f32[1024]{0:T(1024)S(1)}) all-reduce(f32[1024]{0:T(1024)S(1)} %get-tuple-element.109, f32[1024]{0:T(1024)S(1)} %get-tuple-element.108), channel_id=1, replica_groups=mesh['sp'=8,'tp'=4] {'tp'}, use_global_device_ids=true, to_apply=%region_12.13 | all-reduce | flops 2048 | bytes 16384 | tf_op jit(solution)/shard_map/psum | solution.py:186
  373.1 25.1 %all-gather.6.cloned.1.call-done = f32[16,128,256]{2,1,0:T(8,128)} async-done(((f32[2,128,256]{2,1,0:T(8,128)}), f32[16,128,256]{2,1,0:T(8,128)}) %all-gather.6.cloned.1.call-update) | async-done | bytes 2097168 | tf_op jit(solution)/shard_map/all_gather | solution.py:14
  399.0 2.9 multiply_reduce_fusion.2
  402.0 10.6 %fusion.65 = f32[1024,2048]{1,0:T(8,128)} fusion(bf16[256,2048]{1,0:T(8,128)(2,1)S(1)} %copy-done, bf16[1024,2048]{1,0:T(8,128)(2,1)} %all-gather.4.cloned.1.call-done, bf16[2048,256]{1,0:T(8,128)(2,1)} %param.25, f32[1024]{0:T(1024)S(1)} %add_rsqrt_fusion.4, f32[1024,2,128]{2,0,1:T(8,128)} %get-tuple-element.185, f32[128]{0:T(128)S(1)} %copy-done.22, ...), kind=kOutput, calls=%fused_computation.110 | convolution fusion | flops 2150367232 | bytes 15741440 | tf_op jit(solution)/shard_map/dot_general | solution.py:196
  412.6 11.5 %add_convert_fusion = bf16[1024,2048]{1,0:T(8,128)(2,1)} fusion(f32[1024,2048]{1,0:T(8,128)} %fusion.65, bf16[256,2048]{1,0:T(8,128)(2,1)S(1)} %copy-done.26, bf16[1024,2048]{1,0:T(8,128)(2,1)} %all-gather.4.cloned.1.call-done, bf16[2048,256]{1,0:T(8,128)(2,1)} %param.28, f32[1024,256]{1,0:T(8,128)S(1)} %copy-done.8, f32[256]{0:T(256)S(1)} %copy-done.27, ...), kind=kOutput, calls=%fused_computation.28 | convolution fusion | flops 2156134400 | bytes 19937280 | tf_op jit(solution)/shard_map/dot_general | solution.py:198
  424.2 53.2 %reduce-scatter.2.cloned.1.call-done = bf16[256,2048]{1,0:T(8,128)(2,1)} async-done(((bf16[1024,2048]{1,0:T(8,128)(2,1)}), bf16[256,2048]{1,0:T(8,128)(2,1)}) %reduce-scatter.2.cloned.1.call-update) | async-done | bytes 1048592 | tf_op jit(solution)/shard_map/reduce_scatter | solution.py:197
  (218 shorter events, 104.6 us)
Async XLA Ops:
  6.5 395.4 %copy-start = (bf16[256,2048]{1,0:T(8,128)(2,1)S(1)}, bf16[256,2048]{1,0:T(8,128)(2,1)}, u32[]{:S(2)}) copy-start(bf16[256,2048]{1,0:T(8,128)(2,1)} %param.36) | copy-start | bytes 3145732
  6.5 42.8 %copy-start.13 = (bf16[2048,8]{0,1:T(8,128)(2,1)S(1)}, bf16[2048,8]{0,1:T(8,128)(2,1)}, u32[]{:S(2)}) copy-start(bf16[2048,8]{0,1:T(8,128)(2,1)} %param.29) | copy-start | bytes 98308
  6.5 39.6 %all-gather.4.cloned.1.call-start = ((), (), s32[]{:S(2)}) async-start(), calls=%async_computation.1 | async-start | bytes 5242880 | tf_op jit(solution)/shard_map/all_gather | solution.py:85
  7.3 390.9 %all-gather.6.cloned.1.call-start = ((), (), s32[]{:S(2)}) async-start(), calls=%async_computation.3 | async-start | bytes 2359296 | tf_op jit(solution)/shard_map/all_gather | solution.py:14
  7.4 50.4 %copy-start.3 = (f32[2,128,256]{2,1,0:T(8,128)}, f32[2,128,256]{2,1,0:T(8,128)S(1)}, u32[]{:S(2)}) copy-start(f32[2,128,256]{2,1,0:T(8,128)S(1)} %concatenate.15) | copy-start | bytes 786436
  46.1 3.4 copy-start.1
  46.1 4.6 copy-start.14
  49.6 3.2 copy-start.23
  62.4 7.5 %copy-start.12 = (f32[64,64]{1,0:T(8,128)S(1)}, f32[64,64]{1,0:T(8,128)}, u32[]{:S(2)}) copy-start(f32[64,64]{1,0:T(8,128)} %get-tuple-element.189) | copy-start | bytes 49156
  62.4 7.5 %copy-start.16 = (pred[64,64]{1,0:T(8,128)(4,1)S(1)}, pred[64,64]{1,0:T(8,128)(4,1)}, u32[]{:S(2)}) copy-start(pred[64,64]{1,0:T(8,128)(4,1)} %get-tuple-element.187) | copy-start | bytes 12292
  62.4 7.5 %copy-start.17 = (pred[64,64]{1,0:T(8,128)(4,1)S(1)}, pred[64,64]{1,0:T(8,128)(4,1)}, u32[]{:S(2)}) copy-start(pred[64,64]{1,0:T(8,128)(4,1)} %get-tuple-element.188) | copy-start | bytes 12292
  232.4 2.1 copy-start.7
  236.5 4.3 copy-start.15
  238.1 5.8 %copy-start.6 = (f32[2,128,256]{2,1,0:T(8,128)S(1)}, f32[2,128,256]{2,1,0:T(8,128)}, u32[]{:S(2)}) copy-start(f32[2,128,256]{2,1,0:T(8,128)} %copy-done.3) | copy-start | bytes 786436
  243.9 105.0 %copy-start.11 = (bf16[31,256]{1,0:T(8,128)(2,1)S(1)}, bf16[31,256]{1,0:T(8,128)(2,1)}, u32[]{:S(2)}) copy-start(bf16[31,256]{1,0:T(8,128)(2,1)} %param.33) | copy-start | bytes 47620
  243.9 105.1 %copy-start.24 = (bf16[2048,256]{1,0:T(8,128)(2,1)S(1)}, bf16[2048,256]{1,0:T(8,128)(2,1)}, u32[]{:S(2)}) copy-start(bf16[2048,256]{1,0:T(8,128)(2,1)} %param.27) | copy-start | bytes 3145732
  348.9 128.4 %reduce-scatter.2.cloned.1.call-start = ((), (), s32[]{:S(2)}) async-start(), calls=%async_computation.2 | async-start | bytes 5242880 | tf_op jit(solution)/shard_map/reduce_scatter | solution.py:197
  349.0 3.7 copy-start.2
  349.0 3.7 copy-start.25
  354.0 0.8 copy-start.9
  354.8 43.4 %copy-start.4 = (f32[2,128,256]{2,1,0:T(8,128)S(1)}, f32[2,128,256]{2,1,0:T(8,128)}, u32[]{:S(2)}) copy-start(f32[2,128,256]{2,1,0:T(8,128)} %copy-done.3) | copy-start | bytes 786436
  354.8 5.9 %collective-permute-start = (bf16[30,256]{1,0:T(8,128)(2,1)S(1)}, bf16[30,256]{1,0:T(8,128)(2,1)S(1)}, u32[]{:S(2)}, u32[]{:S(2)}) collective-permute-start(bf16[30,256]{1,0:T(8,128)(2,1)S(1)} %slice.292), channel_id=1, source_target_pairs={{0,4},{4,8},{8,12},{12,16},{16,20},{20,24},{24,28},{1,5},{5,9},{9,... | collective-permute-start | bytes 46088 | tf_op jit(solution)/shard_map/ppermute | solution.py:26
  358.9 1.9 copy-start.10
  358.9 1.9 copy-start.18
  358.9 1.9 copy-start.19
  358.9 1.9 copy-start.20
  358.9 1.9 copy-start.21
  398.2 3.8 copy-start.22
  401.9 10.6 %copy-start.8 = (f32[1024,256]{1,0:T(8,128)S(1)}, f32[1024,256]{1,0:T(8,128)}, u32[]{:S(2)}) copy-start(f32[1024,256]{1,0:T(8,128)} %get-tuple-element.138) | copy-start | bytes 3145732
  402.0 10.6 %copy-start.26 = (bf16[256,2048]{1,0:T(8,128)(2,1)S(1)}, bf16[256,2048]{1,0:T(8,128)(2,1)}, u32[]{:S(2)}) copy-start(bf16[256,2048]{1,0:T(8,128)(2,1)} %param.37) | copy-start | bytes 3145732
  402.0 10.6 %copy-start.27 = (f32[256]{0:T(256)S(1)}, f32[256]{0:T(256)}, u32[]{:S(2)}) copy-start(f32[256]{0:T(256)} %param.35) | copy-start | bytes 3076
  402.0 10.6 %copy-start.28 = (f32[256]{0:T(256)S(1)}, f32[256]{0:T(256)}, u32[]{:S(2)}) copy-start(f32[256]{0:T(256)} %param.34) | copy-start | bytes 3076
  (1 other events, 0.7 us)
Sparse Core Ops, SparseCore 0:
  8.9 37.1 all-gather.3
  349.0 49.1 all-gather.5
  424.3 52.9 reduce-scatter.1
where the time goes:
time: 488 us; the launch traced here: 484 us
  other arithmetic  178 us (36%)
  matrix products  139 us (28%)
  waiting for transfers between devices  116 us (24%)
  local copies, waits for them, and re-layouts  27.1 us (6%)
  between operations  13.6 us (3%)
  blocking collectives  6.3 us (1%)
    another operation x4, other arithmetic, block_terms(): jax.scipy.linalg.solve_triangular(identity + lower, right, lower=True, un...  159 us
    reduce_scatter x1, waiting for transfers between devices, local(): lax.psum_scatter((summed + jnp.dot(conv_mixed, out_conv, preferred_elemen...  53.2 us
    all_gather x1, waiting for transfers between devices, local(): piece = lax.all_gather(tokens, 'tp', axis=1, tiled=True)  36.6 us
    dot_general x16, matrix products, advance(): jnp.einsum('hcs,hse->hce', scores_block, fresh, precision=HIGHEST)  28.1 us
    all_gather x1, waiting for transfers between devices, entering(): gathered = lax.all_gather(part, axis)  25.1 us
    dot_general x16, matrix products, advance(): jnp.einsum('hcd,hce->hde', weighted, fresh, precision=HIGHEST)  21.5 us
    dot_general x7, matrix products, local(): jnp.dot(piece, weight, preferred_element_type=jnp.float32)  19.2 us
    dot_general x16, matrix products, advance(): jnp.einsum('hcd,hde->hce', query_block * jnp.exp(log_block)[..., None], m...  18.5 us
  transfers between devices with their start and end apart: 4, of which 3 were waited for; matrix products, arithmetic and copies ran while one was open for 3% of the time, Pallas kernels for 0%

commit v1 on v0

--- a/solution.py
+++ b/solution.py
@@ -7,6 +7,12 @@
 TINY_NORM = 1e-06
 TINY_VAR = 1e-05
 HIGHEST = lax.Precision.HIGHEST
+
+
+def joined_along(parts, dim):
+    shape = list(parts.shape[1:])
+    shape[dim] *= parts.shape[0]
+    return jnp.moveaxis(parts, 0, dim).reshape(shape)
 
 
 def entering(part, axis, combine, identity):
@@ -82,7 +88,19 @@
         w_beta,
         w_decay,
     )
-    piece = lax.all_gather(tokens, "tp", axis=1, tiled=True)
+    count = lax.axis_size("tp")
+    pairs = [(i_2, (i_2 + 1) % count) for i_2 in range(count)]
+    back = [(b, a) for a, b in pairs]
+    lower_2, upper = ([], [])
+    for step in range(count - 1):
+        if step % 2 == 0:
+            lower_2.append(lax.ppermute(lower_2[-1] if lower_2 else tokens, "tp", pairs))
+        else:
+            upper.append(lax.ppermute(upper[-1] if upper else tokens, "tp", back))
+    pieces = jnp.stack([*lower_2[::-1], tokens, *upper])
+    shift = lax.axis_index("tp") - len(lower_2)
+    pieces = pieces[(jnp.arange(count) - shift) % count]
+    piece = joined_along(pieces, 1)
     totals = tuple(
         (jnp.dot(piece, weight, preferred_element_type=jnp.float32) for weight in weights)
     )

time: 488 us -> 508 us (1.041)
  local copies, waits for them, and re-layouts: 27.1 us -> 38.6 us
  starting transfers between devices: 3.58 us -> 10.2 us
    all_gather x1 -> x0, waiting for transfers between devices: 36.6 us -> none  [local(): piece = lax.all_gather(tokens, 'tp', axis=1, tiled=True)]
    ppermute x0 -> x3, waiting for transfers between devices: none -> 30.9 us  [the longest x2 30.9 us: local(): lax.ppermute(lower_2[-1] if lower_2 else tokens, 'tp', pairs)]
    transpose x0 -> x1, local copies, waits for them, and re-layouts: none -> 6.3 us  [joined_along(): return jnp.moveaxis(parts, 0, dim).reshape(shape)]
  transfers between devices with their start and end apart: 4 -> 6, of which waited for: 3 -> 4; matrix products, arithmetic and copies ran while one was open for 3% -> 3% of each run, Pallas kernels for 0% -> 0%
where the time goes in v1:
time: 508 us; the launch traced here: 503 us
  other arithmetic  182 us (36%)
  matrix products  141 us (28%)
  waiting for transfers between devices  112 us (22%)
  local copies, waits for them, and re-layouts  38.6 us (8%)
  between operations  13.8 us (3%)
  starting transfers between devices  10.2 us (2%)
  blocking collectives  6.04 us (1%)
    another operation x4, other arithmetic, block_terms(): jax.scipy.linalg.solve_triangular(identity + lower, right, lower=True, un...  159 us
    reduce_scatter x1, waiting for transfers between devices, local(): lax.psum_scatter((summed + jnp.dot(conv_mixed, out_conv, preferred_elemen...  53.4 us
    ppermute x2, waiting for transfers between devices, local(): lax.ppermute(lower_2[-1] if lower_2 else tokens, 'tp', pairs)  30.9 us
    dot_general x16, matrix products, advance(): jnp.einsum('hcs,hse->hce', scores_block, fresh, precision=HIGHEST)  28.1 us
    all_gather x1, waiting for transfers between devices, entering(): gathered = lax.all_gather(part, axis)  27.6 us
    dot_general x16, matrix products, advance(): jnp.einsum('hcd,hce->hde', weighted, fresh, precision=HIGHEST)  21.5 us
    dot_general x7, matrix products, local(): jnp.dot(piece, weight, preferred_element_type=jnp.float32)  20.8 us
    dot_general x16, matrix products, advance(): jnp.einsum('hcd,hde->hce', query_block * jnp.exp(log_block)[..., None], m...  18.5 us
  transfers between devices with their start and end apart: 6, of which 4 were waited for; matrix products, arithmetic and copies ran while one was open for 3% of the time, Pallas kernels for 0%

profile of v1, /device:TPU:0, one launch (start us, length us, event | category | flops | bytes accessed | tf_op | source)
XLA Modules:
  0.0 503.3 jit_solution(6929417415715291817)
XLA Ops:
  7.0 1.9 collective-permute-start.2
  9.0 21.3 %collective-permute-done = bf16[1024,512]{1,0:T(8,128)(2,1)S(1)} collective-permute-done((bf16[1024,512]{1,0:T(8,128)(2,1)}, bf16[1024,512]{1,0:T(8,128)(2,1)S(1)}, u32[]{:S(2)}, u32[]{:S(2)}) %collective-permute-start) | collective-permute-done | bytes 1048608 | tf_op jit(solution)/shard_map/ppermute | solution.py:97
  30.3 2.6 collective-permute-start.1
  35.1 9.5 %collective-permute-done.1 = bf16[1024,512]{1,0:T(8,128)(2,1)} collective-permute-done((bf16[1024,512]{1,0:T(8,128)(2,1)S(1)}, bf16[1024,512]{1,0:T(8,128)(2,1)}, u32[]{:S(2)}, u32[]{:S(2)}) %collective-permute-start.1) | collective-permute-done | bytes 1048608 | tf_op jit(solution)/shard_map/ppermute | solution.py:97
  44.6 3.4 pad_maximum_fusion
  48.0 5.0 gather_fusion
  53.0 3.1 multiply_reduce_fusion
  56.1 6.3 %copy.67 = bf16[1024,4,512]{0,2,1:T(8,128)(2,1)} copy(bf16[1024,4,512]{2,0,1:T(8,128)(2,1)} %bitcast.194) | data formatting | bytes 8388608 | tf_op jit(solution)/shard_map/transpose | solution.py:15
  62.5 3.0 fusion.147
  67.2 3.5 fusion.47
  71.6 3.8 fusion.45
  76.9 4.8 fusion.43
  84.5 3.7 fusion.39
  88.2 158.7 %custom-call.4 = f32[2,16,1,64,64]{3,4,2,1,0:T(8,128)} custom-call(f32[2,16,1,64,64]{4,3,2,1,0:T(8,128)} %fusion.39), custom_call_target="InvertDiagBlocksLowerTriangular" | custom-call | tf_op jit(solution)/shard_map/jit(_solve_triangular)/vmap(vmap())/triangular_solve | solution.py:50
  246.9 2.3 bitcast_multiply_fusion.7
  249.2 2.0 fusion.16
  255.5 3.1 fusion.26
  258.6 104.3 %while.22 = (s32[]{:T(128)}, f32[2,128,256]{2,1,0:T(8,128)S(1)}, f32[16,2,64,256]{3,2,1,0:T(8,128)}, f32[16,2,64]{2,0,1:T(8,128)S(1)}, f32[16,2,64,128]{3,2,1,0:...) while((s32[]{:T(128)}, f32[2,128,256]{2,1,0:T(8,128)S(1)}, ...), condition=%wide.region_5.6_spmd, body=%wide.region_4.5_spmd.sunk | while | flops 176390272 | bytes 2298537 | solution.py:166
  269.9 1.8 fusion.192
  276.5 1.8 fusion.192
  283.0 1.8 fusion.192
  361.2 1.8 fusion.192
  363.8 3.8 fusion.58
  369.8 5.1 %collective-permute-start.3 = (bf16[30,256]{1,0:T(8,128)(2,1)S(1)}, bf16[30,256]{1,0:T(8,128)(2,1)S(1)}, u32[]{:S(2)}, u32[]{:S(2)}) collective-permute-start(bf16[30,256]{1,0:T(8,128)(2,1)S(1)} %slice.294), channel_id=1, source_target_pairs={{0,4},{4,8},{8,12},{12,16},{16,20},{20,24},{24,28},{1,5},{5,9},{9,... | collective-permute-start | bytes 46088 | tf_op jit(solution)/shard_map/ppermute | solution.py:32
  375.5 1.9 copy.80
  377.5 6.0 %fusion.144 = (f32[1024]{0:T(1024)S(1)}, f32[1024]{0:T(1024)S(1)}, f32[1024,256]{1,0:T(8,128)}) fusion(f32[256]{0:T(256)S(1)} %bitcast.237, bf16[1024,256]{1,0:T(8,128)(2,1)S(1)} %copy-done.10, f32[256]{0:T(256)S(1)} %bitcast.238, bf16[30,256]{1,0:T(8,128)(2,1)S(1)} %collective-permute-done.3, f32[256]{0:T(256)S(1)} %bitcast.209, f32[256]{0:T(256)S(1)} %bitcast.210, ...), kind=kLoop, calls=%fused_computation.261 | loop fusion | flops 48494592 | bytes 1628160 | tf_op jit(solution)/shard_map/reduce_sum | solution.py:202
  383.4 6.0 %all-reduce.3 = (f32[1024]{0:T(1024)S(1)}, f32[1024]{0:T(1024)S(1)}) all-reduce(f32[1024]{0:T(1024)S(1)} %get-tuple-element.118, f32[1024]{0:T(1024)S(1)} %get-tuple-element.117), channel_id=1, replica_groups=mesh['sp'=8,'tp'=4] {'tp'}, use_global_device_ids=true, to_apply=%region_12.13 | all-reduce | flops 2048 | bytes 16384 | tf_op jit(solution)/shard_map/psum | solution.py:204
  389.5 27.6 %all-gather.3.cloned.1.call-done = f32[16,128,256]{2,1,0:T(8,128)} async-done(((f32[2,128,256]{2,1,0:T(8,128)}), f32[16,128,256]{2,1,0:T(8,128)}) %all-gather.3.cloned.1.call-update) | async-done | bytes 2097168 | tf_op jit(solution)/shard_map/all_gather | solution.py:20
  417.9 2.9 multiply_reduce_fusion.2
  420.9 10.6 %fusion.65 = f32[1024,2048]{1,0:T(8,128)} fusion(bf16[256,2048]{1,0:T(8,128)(2,1)S(1)} %copy-done, bf16[1024,2048]{0,1:T(8,128)(2,1)} %bitcast.190, bf16[2048,256]{1,0:T(8,128)(2,1)} %param.25, f32[1024]{0:T(1024)S(1)} %add_rsqrt_fusion.4, f32[1024,2,128]{2,0,1:T(8,128)} %get-tuple-element.194, f32[128]{0:T(128)S(1)} %copy-done.28, ...), kind=kOutput, calls=%fused_computation.112 | convolution fusion | flops 2150367232 | bytes 15741440 | tf_op jit(solution)/shard_map/dot_general | solution.py:214
  431.5 11.5 %add_convert_fusion = bf16[1024,2048]{1,0:T(8,128)(2,1)} fusion(f32[1024,2048]{1,0:T(8,128)} %fusion.65, bf16[256,2048]{1,0:T(8,128)(2,1)S(1)} %copy-done.25, bf16[1024,2048]{0,1:T(8,128)(2,1)} %bitcast.191, bf16[2048,256]{1,0:T(8,128)(2,1)} %param.28, f32[1024,256]{1,0:T(8,128)S(1)} %copy-done.8, f32[256]{0:T(256)S(1)} %copy-done.26, ...), kind=kOutput, calls=%fused_computation.29 | convolution fusion | flops 2156134400 | bytes 19937280 | tf_op jit(solution)/shard_map/dot_general | solution.py:216
  443.1 53.4 %reduce-scatter.2.cloned.1.call-done = bf16[256,2048]{1,0:T(8,128)(2,1)} async-done(((bf16[1024,2048]{1,0:T(8,128)(2,1)}), bf16[256,2048]{1,0:T(8,128)(2,1)}) %reduce-scatter.2.cloned.1.call-update) | async-done | bytes 1048592 | tf_op jit(solution)/shard_map/reduce_scatter | solution.py:215
  (226 shorter events, 115.1 us)
Async XLA Ops:
  6.5 414.3 %copy-start = (bf16[256,2048]{1,0:T(8,128)(2,1)S(1)}, bf16[256,2048]{1,0:T(8,128)(2,1)}, u32[]{:S(2)}) copy-start(bf16[256,2048]{1,0:T(8,128)(2,1)} %param.36) | copy-start | bytes 3145732
  6.5 410.5 %all-gather.3.cloned.1.call-start = ((), (), s32[]{:S(2)}) async-start(), calls=%async_computation.2 | async-start | bytes 2359296 | tf_op jit(solution)/shard_map/all_gather | solution.py:20
  6.5 23.8 %collective-permute-start = (bf16[1024,512]{1,0:T(8,128)(2,1)}, bf16[1024,512]{1,0:T(8,128)(2,1)S(1)}, u32[]{:S(2)}, u32[]{:S(2)}) collective-permute-start(bf16[1024,512]{1,0:T(8,128)(2,1)} %param.21), channel_id=1, source_target_pairs={{0,1},{1,2},{2,3},{3,0},{4,5},{5,6},{6,7},{7,4},{8,9},{9,10},{10,1... | collective-permute-start | bytes 3145736 | tf_op jit(solution)/shard_map/ppermute | solution.py:97
  7.0 28.1 %collective-permute-start.2 = (bf16[1024,512]{1,0:T(8,128)(2,1)}, bf16[1024,512]{1,0:T(8,128)(2,1)S(1)}, u32[]{:S(2)}, u32[]{:S(2)}) collective-permute-start(bf16[1024,512]{1,0:T(8,128)(2,1)} %param.21), channel_id=1, source_target_pairs={{1,0},{2,1},{3,2},{0,3},{5,4},{6,5},{7,6},{4,7},{9,8},{10,9},{11,1... | collective-permute-start | bytes 3145736 | tf_op jit(solution)/shard_map/ppermute | solution.py:99
  30.3 14.3 %collective-permute-start.1 = (bf16[1024,512]{1,0:T(8,128)(2,1)S(1)}, bf16[1024,512]{1,0:T(8,128)(2,1)}, u32[]{:S(2)}, u32[]{:S(2)}) collective-permute-start(bf16[1024,512]{1,0:T(8,128)(2,1)S(1)} %collective-permute-done), channel_id=1, source_target_pairs={{0,1},{1,2},{2,3},{3,0},{4,5},{5,6},{6,7},{7,4},{8,9},{9,10},{10,1... | collective-permute-start | bytes 3145736 | tf_op jit(solution)/shard_map/ppermute | solution.py:97
  33.0 29.4 %copy-start.1 = (f32[2,128,256]{2,1,0:T(8,128)}, f32[2,128,256]{2,1,0:T(8,128)S(1)}, u32[]{:S(2)}) copy-start(f32[2,128,256]{2,1,0:T(8,128)S(1)} %concatenate.15) | copy-start | bytes 786436
  56.1 6.3 %copy-start.12 = (bf16[2048,8]{0,1:T(8,128)(2,1)S(1)}, bf16[2048,8]{0,1:T(8,128)(2,1)}, u32[]{:S(2)}) copy-start(bf16[2048,8]{0,1:T(8,128)(2,1)} %param.29) | copy-start | bytes 98308
  62.4 3.4 copy-start.5
  62.4 3.5 copy-start.13
  62.4 4.8 copy-start.22
  76.9 7.5 %copy-start.14 = (f32[64,64]{1,0:T(8,128)S(1)}, f32[64,64]{1,0:T(8,128)}, u32[]{:S(2)}) copy-start(f32[64,64]{1,0:T(8,128)} %get-tuple-element.198) | copy-start | bytes 49156
  76.9 7.5 %copy-start.16 = (pred[64,64]{1,0:T(8,128)(4,1)S(1)}, pred[64,64]{1,0:T(8,128)(4,1)}, u32[]{:S(2)}) copy-start(pred[64,64]{1,0:T(8,128)(4,1)} %get-tuple-element.196) | copy-start | bytes 12292
  76.9 7.5 %copy-start.17 = (pred[64,64]{1,0:T(8,128)(4,1)S(1)}, pred[64,64]{1,0:T(8,128)(4,1)}, u32[]{:S(2)}) copy-start(pred[64,64]{1,0:T(8,128)(4,1)} %get-tuple-element.197) | copy-start | bytes 12292
  246.9 2.3 copy-start.7
  251.2 4.3 copy-start.15
  252.9 5.8 %copy-start.4 = (f32[2,128,256]{2,1,0:T(8,128)S(1)}, f32[2,128,256]{2,1,0:T(8,128)}, u32[]{:S(2)}) copy-start(f32[2,128,256]{2,1,0:T(8,128)} %copy-done.1) | copy-start | bytes 786436
  258.6 105.1 %copy-start.11 = (bf16[31,256]{1,0:T(8,128)(2,1)S(1)}, bf16[31,256]{1,0:T(8,128)(2,1)}, u32[]{:S(2)}) copy-start(bf16[31,256]{1,0:T(8,128)(2,1)} %param.33) | copy-start | bytes 47620
  258.6 105.1 %copy-start.23 = (bf16[2048,256]{1,0:T(8,128)(2,1)S(1)}, bf16[2048,256]{1,0:T(8,128)(2,1)}, u32[]{:S(2)}) copy-start(bf16[2048,256]{1,0:T(8,128)(2,1)} %param.27) | copy-start | bytes 3145732
  363.7 132.8 %reduce-scatter.2.cloned.1.call-start = ((), (), s32[]{:S(2)}) async-start(), calls=%async_computation.1 | async-start | bytes 5242880 | tf_op jit(solution)/shard_map/reduce_scatter | solution.py:215
  363.8 3.8 copy-start.6
  363.8 3.8 copy-start.24
  369.8 47.3 %copy-start.2 = (f32[2,128,256]{2,1,0:T(8,128)S(1)}, f32[2,128,256]{2,1,0:T(8,128)}, u32[]{:S(2)}) copy-start(f32[2,128,256]{2,1,0:T(8,128)} %copy-done.1) | copy-start | bytes 786436
  369.8 7.7 %collective-permute-start.3 = (bf16[30,256]{1,0:T(8,128)(2,1)S(1)}, bf16[30,256]{1,0:T(8,128)(2,1)S(1)}, u32[]{:S(2)}, u32[]{:S(2)}) collective-permute-start(bf16[30,256]{1,0:T(8,128)(2,1)S(1)} %slice.294), channel_id=1, source_target_pairs={{0,4},{4,8},{8,12},{12,16},{16,20},{20,24},{24,28},{1,5},{5,9},{9,... | collective-permute-start | bytes 46088 | tf_op jit(solution)/shard_map/ppermute | solution.py:32
  375.5 1.9 copy-start.18
  375.5 2.0 copy-start.19
  375.5 2.0 copy-start.20
  375.5 2.0 copy-start.21
  417.1 3.8 copy-start.28
  420.9 10.7 %copy-start.8 = (f32[1024,256]{1,0:T(8,128)S(1)}, f32[1024,256]{1,0:T(8,128)}, u32[]{:S(2)}) copy-start(f32[1024,256]{1,0:T(8,128)} %get-tuple-element.147) | copy-start | bytes 3145732
  420.9 10.6 %copy-start.25 = (bf16[256,2048]{1,0:T(8,128)(2,1)S(1)}, bf16[256,2048]{1,0:T(8,128)(2,1)}, u32[]{:S(2)}) copy-start(bf16[256,2048]{1,0:T(8,128)(2,1)} %param.37) | copy-start | bytes 3145732
  420.9 10.6 %copy-start.26 = (f32[256]{0:T(256)S(1)}, f32[256]{0:T(256)}, u32[]{:S(2)}) copy-start(f32[256]{0:T(256)} %param.35) | copy-start | bytes 3076
  420.9 10.6 %copy-start.27 = (f32[256]{0:T(256)S(1)}, f32[256]{0:T(256)}, u32[]{:S(2)}) copy-start(f32[256]{0:T(256)} %param.34) | copy-start | bytes 3076
  (3 other events, 3.4 us)
Sparse Core Ops, SparseCore 0:
  363.8 53.2 all-gather.2
  443.2 53.2 reduce-scatter.1
